TPU v7x, 32 devices: a whole 2x2x4 slice. The times are simulated.
32 devices in a mesh: ep: 8 (over z, x), tp: 4 (over y, core).
Axes of the slice: x: 2, y: 2, z: 4, core: 2. Of those that a mesh axis runs over, the one named last changes fastest.
Arguments:
- tokens: bfloat16 [192, 3072], P('ep'), may hold values from -6 to 6
- norm_gain: float32 [3072], replicated, may hold values from 0.1 to 1.9
- routing: int32 [192, 4], P('ep'), may hold values from 0 to 7, all different within a row; in each aligned block of 24 rows (0 to 23, 24 to 47, ...) at most 13 rows name the same one
- route_weight: float32 [192, 4], P('ep'), may hold values from 0.05 to 1
- w_gate: bfloat16 [8, 3072, 3072], P('ep', None, 'tp'), may hold values from -0.3125 to 0.3125
- w_up: bfloat16 [8, 3072, 3072], P('ep', None, 'tp'), may hold values from -0.3125 to 0.3125
- w_down: bfloat16 [8, 3072, 3072], P('ep', 'tp'), may hold values from -0.01953125 to 0.01953125
Outputs:
- mixed: bfloat16 [192, 3072], P('ep', 'tp')
Inputs may be any that keep to these rules, and one draw needn't show every extreme that they name: `routing`: each row names 4 different experts. Within the rows of one device (aligned blocks of 24 rows) no expert is named by more than 13 rows, a bound that some block reaches.
All inputs are finite; a program needn't handle non-finite values.
Results may differ from a plain program's by a relative error of at most 0.019.
Values may be sent and summed in bfloat16 or wider, within the bound.
No kernel may reach another device: no remote copies, remote signals or barrier semaphores. Data moves between devices by JAX's collectives and lax.ppermute only.
A program may use at most 64 MiB of HBM per device.

v0:
```python
import jax
import jax.numpy as jnp
from jax import lax
from jax.sharding import PartitionSpec as P

NORM_EPS = 1e-06
CLAMP_LIMIT = 7.0
SIGMOID_SCALE = 1.702


def slot_index(route_rows, expert_total, capacity):
    flat_ids = route_rows.reshape(-1)
    one_hot = (flat_ids[:, None] == jnp.arange(expert_total, dtype=jnp.int32)[None, :]).astype(
        jnp.int32
    )
    before = jnp.cumsum(one_hot, axis=0) - one_hot
    ranked = jnp.sum(before * one_hot, axis=1)
    return flat_ids * capacity + ranked


def local(tokens, norm_gain, routing, route_weight, w_gate, w_up, w_down):
    tok_count = tokens.shape[0]
    width = tokens.shape[1]
    top_count = routing.shape[1]
    expert_total = lax.axis_size("ep") * w_gate.shape[0]
    capacity = max(2, tok_count * top_count // expert_total + 1)
    slice_width = width // lax.axis_size("tp")
    values = tokens.astype(jnp.float32)
    scaled = values * lax.rsqrt(jnp.mean(values * values, axis=-1, keepdims=True) + NORM_EPS)
    normal = (scaled * norm_gain).astype(jnp.bfloat16)
    dest = slot_index(routing, expert_total, capacity)
    slot_ids = jnp.arange(expert_total * capacity, dtype=jnp.int32)
    select = jnp.sum(dest.reshape(1, tok_count, top_count) == slot_ids[:, None, None], axis=2)
    sending = jnp.dot(
        select.astype(jnp.bfloat16), normal, preferred_element_type=jnp.float32
    ).astype(jnp.bfloat16)
    gate_mat = w_gate[0]
    up_mat = w_up[0]
    down_mat = w_down[0]
    own_share = lax.dynamic_slice_in_dim(
        sending, lax.axis_index("tp") * slice_width, slice_width, 1
    )
    arrived = lax.all_to_all(own_share, "ep", split_axis=0, concat_axis=0, tiled=True)
    pieces = lax.all_gather(arrived, "tp", axis=1, tiled=True)
    gate_pre = jnp.dot(pieces, gate_mat, preferred_element_type=jnp.float32)
    up_pre = jnp.dot(pieces, up_mat, preferred_element_type=jnp.float32)
    gated = jnp.minimum(gate_pre, CLAMP_LIMIT)
    upper = jnp.clip(up_pre, -CLAMP_LIMIT, CLAMP_LIMIT)
    hidden = ((upper + 1.0) * gated * jax.nn.sigmoid(SIGMOID_SCALE * gated)).astype(jnp.bfloat16)
    summed = lax.psum_scatter(
        lax.dot_general(
            down_mat, hidden, (((0,), (1,)), ((), ())), preferred_element_type=jnp.float32
        ).astype(jnp.bfloat16),
        "tp",
        scatter_dimension=0,
        tiled=True,
    )
    back = lax.all_to_all(summed, "ep", split_axis=1, concat_axis=1, tiled=True)
    picked = back[:, dest].reshape(slice_width, tok_count, top_count)
    mixed = jnp.sum(picked.astype(jnp.float32) * route_weight[None, :, :], axis=2)
    return mixed.T.astype(jnp.bfloat16)


def solution(mesh):
    placed = (
        P("ep", None),
        P(),
        P("ep", None),
        P("ep", None),
        P("ep", None, "tp"),
        P("ep", None, "tp"),
        P("ep", "tp", None),
    )
    return jax.shard_map(
        local, mesh=mesh, in_specs=placed, out_specs=P("ep", "tp"), check_vma=False
    )
```

profile of v0, /device:TPU:0, one launch (start us, length us, event | category | flops | bytes accessed | tf_op | source)
XLA Modules:
  0.0 87.3 jit_solution(828306079801427838)
XLA Ops:
  6.5 0.0 reduce-scatter.2.cloned.1.call-start
  6.5 0.8 copy.14
  7.3 0.1 eq.28
  7.4 0.1 fusion.48
  7.5 0.1 reduce_window_sum.11
  7.6 0.2 select_reduce_fusion
  7.8 0.1 reduce_sum.41
  7.9 0.1 copy.16
  8.0 0.1 convert_reduce_fusion
  8.1 1.0 %fusion.37 = f32[24]{0:T(128)S(1)} fusion(bf16[24,3072]{1,0:T(8,128)(2,1)} %param.7), kind=kLoop, calls=%fused_computation.23 | loop fusion | flops 221160 | bytes 147552 | tf_op jit(solution)/shard_map/reduce_sum | solution.py:29
  9.2 1.3 %fusion.44 = bf16[104,3072]{1,0:T(8,128)(2,1)S(1)} fusion(bf16[24,3072]{1,0:T(8,128)(2,1)} %param.7, f32[3072]{0:T(1024)} %param.8, f32[24]{0:T(128)S(1)} %add_rsqrt_fusion, s32[104,24]{0,1:T(8,128)S(1)} %convert_reduce_fusion), kind=kOutput, calls=%fused_computation.32 | convolution fusion | flops 15632832 | bytes 808800 | tf_op jit(solution)/shard_map/dot_general | solution.py:34
  10.5 0.1 all_to_all.16
  10.6 15.0 %all_to_all.24 = bf16[8,13,768]{2,1,0:T(8,128)(2,1)S(1)} all-to-all(bf16[8,13,768]{2,1,0:T(8,128)(2,1)S(1)} %all_to_all.16), channel_id=1, replica_groups=mesh['ep'=8,'tp'=4] {'ep'}, dimensions={0} | all-to-all | bytes 319488 | tf_op jit(solution)/shard_map/all_to_all | solution.py:43
  25.6 0.1 all_to_all.18
  25.7 7.8 %all_gather.3 = bf16[104,3072]{1,0:T(8,128)(2,1)S(1)} all-gather(bf16[104,768]{1,0:T(8,128)(2,1)S(1)} %all_to_all.18), channel_id=1, replica_groups=mesh['ep'=8,'tp'=4] {'tp'}, dimensions={1}, use_global_device_ids=true | all-gather | bytes 798720 | tf_op jit(solution)/shard_map/all_gather | solution.py:44
  33.5 3.2 %fusion.12 = f32[104,768]{1,0:T(8,128)S(1)} fusion(bf16[104,3072]{1,0:T(8,128)(2,1)S(1)} %all_gather.3, bf16[1,3072,768]{2,1,0:T(8,128)(2,1)} %param.11), kind=kOutput, calls=%fused_computation.9 | convolution fusion | flops 490813440 | bytes 5677056 | tf_op jit(solution)/shard_map/dot_general | solution.py:45
  36.7 0.0 copy-start
  36.7 6.5 %fusion.9 = bf16[3072,104]{0,1:T(8,128)(2,1)} fusion(bf16[1,768,3072]{2,1,0:T(8,128)(2,1)} %param.13, f32[104,768]{1,0:T(8,128)S(1)} %fusion.12, bf16[104,3072]{1,0:T(8,128)(2,1)S(1)} %all_gather.3, bf16[1,3072,768]{2,1,0:T(8,128)(2,1)} %param.12), kind=kOutput, calls=%fused_computation.8 | convolution fusion | flops 982505472 | bytes 11034624 | tf_op jit(solution)/shard_map/dot_general | solution.py:51
  43.2 0.0 reduce-scatter.2.cloned.1.call-update
  43.2 0.1 mul.76
  43.3 0.0 copy-done
  43.4 0.1 copy.17
  43.4 20.2 %reduce-scatter.2.cloned.1.call-done = bf16[768,104]{0,1:T(8,128)(2,1)} async-done(((bf16[3072,104]{0,1:T(8,128)(2,1)}), bf16[768,104]{0,1:T(8,128)(2,1)}) %reduce-scatter.2.cloned.1.call-update) | async-done | bytes 159760 | tf_op jit(solution)/shard_map/reduce_scatter | solution.py:50
  63.7 1.6 %all_to_all.19 = bf16[768,8,13]{0,2,1:T(8,128)(2,1)} reshape(bf16[768,104]{0,1:T(8,128)(2,1)} %reduce-scatter.2.cloned.1.call-done) | data formatting | bytes 319488 | tf_op jit(solution)/shard_map/all_to_all | solution.py:58
  65.3 5.5 %all-to-all-start.1 = ((bf16[768,8,13]{0,2,1:T(8,128)(2,1)}), bf16[768,8,13]{0,2,1:T(8,128)(2,1)S(1)}, u32[]{:S(2)}, u32[]{:S(2)}) async-start(bf16[768,8,13]{0,2,1:T(8,128)(2,1)} %all_to_all.19), calls=%async_computation.2 | async-start | bytes 393216 | tf_op jit(solution)/shard_map/all_to_all | solution.py:58
  70.8 7.8 %all-to-all-done.1 = bf16[768,8,13]{0,2,1:T(8,128)(2,1)S(1)} async-done(((bf16[768,8,13]{0,2,1:T(8,128)(2,1)}), bf16[768,8,13]{0,2,1:T(8,128)(2,1)S(1)}, u32[]{:S(2)}, u32[]{:S(2)}) %all-to-all-start.1) | async-done | bytes 159776 | tf_op jit(solution)/shard_map/all_to_all | solution.py:58
  78.6 0.1 all_to_all.21
  78.7 0.8 gather_fusion
  79.5 0.1 reshape.54
  79.6 0.9 multiply_reduce_fusion
  (6 shorter events, 0.1 us)
Async XLA Ops:
  6.5 57.1 %reduce-scatter.2.cloned.1.call-start = ((), (), s32[]{:S(2)}) async-start(), calls=%async_computation.3 | async-start | bytes 798720 | tf_op jit(solution)/shard_map/reduce_scatter | solution.py:50
  36.7 6.7 %copy-start = (f32[24,4]{0,1:T(4,128)S(1)}, f32[24,4]{0,1:T(4,128)}, u32[]{:S(2)}) copy-start(f32[24,4]{0,1:T(4,128)} %param.10) | copy-start | bytes 1156
  65.3 13.3 %all-to-all-start.1 = ((bf16[768,8,13]{0,2,1:T(8,128)(2,1)}), bf16[768,8,13]{0,2,1:T(8,128)(2,1)S(1)}, u32[]{:S(2)}, u32[]{:S(2)}) async-start(bf16[768,8,13]{0,2,1:T(8,128)(2,1)} %all_to_all.19), calls=%async_computation.2 | async-start | bytes 393216 | tf_op jit(solution)/shard_map/all_to_all | solution.py:58
Sparse Core Ops, SparseCore 0:
  43.4 20.2 reduce-scatter.1
where the time goes:
time: 87.7 us; the launch traced here: 87.3 us
  waiting for transfers between devices  28 us (32%)
  blocking collectives  22.9 us (26%)
  between operations  13.5 us (15%)
  matrix products  11 us (13%)
  starting transfers between devices  5.5 us (6%)
  local copies, waits for them, and re-layouts  3.96 us (5%)
  other arithmetic  2.44 us (3%)
    reduce_scatter x1, waiting for transfers between devices, local(): lax.psum_scatter(lax.dot_general(down_mat, hidden, (((0,), (1,)), ((), ()...  20.2 us
    all_to_all x1, blocking collectives, local(): lax.all_to_all(own_share, 'ep', split_axis=0, concat_axis=0, tiled=True)  15 us
    all_gather x1, blocking collectives, local(): pieces = lax.all_gather(arrived, 'tp', axis=1, tiled=True)  7.82 us
    all_to_all x1, waiting for transfers between devices, local(): back = lax.all_to_all(summed, 'ep', split_axis=1, concat_axis=1, tiled=True)  7.77 us
    dot_general x1, matrix products, local(): lax.dot_general(down_mat, hidden, (((0,), (1,)), ((), ())), preferred_ele...  6.54 us
    all_to_all x1, starting transfers between devices, local(): back = lax.all_to_all(summed, 'ep', split_axis=1, concat_axis=1, tiled=True)  5.5 us
    dot_general x1, matrix products, local(): gate_pre = jnp.dot(pieces, gate_mat, preferred_element_type=jnp.float32)  3.18 us
  transfers between devices with their start and end apart: 2, of which 2 were waited for; matrix products, arithmetic and copies ran while one was open for 0% of the time, Pallas kernels for 0%

commit v1 on v0

--- a/solution.py
+++ b/solution.py
@@ -55,7 +55,11 @@
         scatter_dimension=0,
         tiled=True,
     )
-    back = lax.all_to_all(summed, "ep", split_axis=1, concat_axis=1, tiled=True)
+    r1 = jax.lax.axis_size("ep")
+    outer = jnp.split(summed, r1, 1)
+    f_next = jnp.stack(outer, axis=0)
+    found_now = jax.lax.all_to_all(f_next, "ep", split_axis=0, concat_axis=0)
+    back = jnp.concatenate(found_now, 1)
     picked = back[:, dest].reshape(slice_width, tok_count, top_count)
     mixed = jnp.sum(picked.astype(jnp.float32) * route_weight[None, :, :], axis=2)
     return mixed.T.astype(jnp.bfloat16)

time: 87.7 us -> 97.5 us (1.11)
  local copies, waits for them, and re-layouts: 3.96 us -> 13.3 us
    unnamed x4 -> x11, local copies, waits for them, and re-layouts: 0.85 us -> 10.5 us
    all_to_all x2 -> x0, local copies, waits for them, and re-layouts: 1.71 us -> none  [local(): back = lax.all_to_all(summed, 'ep', split_axis=1, concat_axis=1, tiled=True)]
    another operation x0 -> x1, local copies, waits for them, and re-layouts: none -> 1.35 us  [local(): f_next = jnp.stack(outer, axis=0)]
where the time goes in v1:
time: 97.5 us; the launch traced here: 96.6 us
  waiting for transfers between devices  28 us (29%)
  blocking collectives  22.9 us (23%)
  between operations  13.5 us (14%)
  local copies, waits for them, and re-layouts  13.3 us (14%)
  matrix products  11 us (11%)
  starting transfers between devices  5.5 us (6%)
  other arithmetic  2.44 us (3%)
    reduce_scatter x1, waiting for transfers between devices, local(): lax.psum_scatter(lax.dot_general(down_mat, hidden, (((0,), (1,)), ((), ()...  20.2 us
    all_to_all x1, blocking collectives, local(): lax.all_to_all(own_share, 'ep', split_axis=0, concat_axis=0, tiled=True)  15 us
    unnamed x11, local copies, waits for them, and re-layouts  10.5 us
    all_gather x1, blocking collectives, local(): pieces = lax.all_gather(arrived, 'tp', axis=1, tiled=True)  7.82 us
    all_to_all x1, waiting for transfers between devices, local(): found_now = jax.lax.all_to_all(f_next, 'ep', split_axis=0, concat_axis=0)  7.77 us
    dot_general x1, matrix products, local(): lax.dot_general(down_mat, hidden, (((0,), (1,)), ((), ())), preferred_ele...  6.54 us
    all_to_all x1, starting transfers between devices, local(): found_now = jax.lax.all_to_all(f_next, 'ep', split_axis=0, concat_axis=0)  5.5 us
    dot_general x1, matrix products, local(): gate_pre = jnp.dot(pieces, gate_mat, preferred_element_type=jnp.float32)  3.18 us
  transfers between devices with their start and end apart: 2, of which 2 were waited for; matrix products, arithmetic and copies ran while one was open for 0% of the time, Pallas kernels for 0%

profile of v1, /device:TPU:0, one launch (start us, length us, event | category | flops | bytes accessed | tf_op | source)
XLA Modules:
  0.0 96.6 jit_solution(892729293245453577)
XLA Ops:
  6.5 0.0 reduce-scatter.2.cloned.1.call-start
  6.5 0.8 copy.14
  7.3 0.1 eq.28
  7.4 0.1 fusion.48
  7.5 0.1 reduce_window_sum.11
  7.6 0.2 select_reduce_fusion
  7.8 0.1 reduce_sum.41
  7.9 0.1 copy.16
  8.0 0.1 convert_reduce_fusion
  8.1 1.0 %fusion.37 = f32[24]{0:T(128)S(1)} fusion(bf16[24,3072]{1,0:T(8,128)(2,1)} %param.7), kind=kLoop, calls=%fused_computation.23 | loop fusion | flops 221160 | bytes 147552 | tf_op jit(solution)/shard_map/reduce_sum | solution.py:29
  9.2 1.3 %fusion.44 = bf16[104,3072]{1,0:T(8,128)(2,1)S(1)} fusion(bf16[24,3072]{1,0:T(8,128)(2,1)} %param.7, f32[3072]{0:T(1024)} %param.8, f32[24]{0:T(128)S(1)} %add_rsqrt_fusion, s32[104,24]{0,1:T(8,128)S(1)} %convert_reduce_fusion), kind=kOutput, calls=%fused_computation.32 | convolution fusion | flops 15632832 | bytes 808800 | tf_op jit(solution)/shard_map/dot_general | solution.py:34
  10.5 0.1 all_to_all.11
  10.6 15.0 %all_to_all.17 = bf16[8,13,768]{2,1,0:T(8,128)(2,1)S(1)} all-to-all(bf16[8,13,768]{2,1,0:T(8,128)(2,1)S(1)} %all_to_all.11), channel_id=1, replica_groups=mesh['ep'=8,'tp'=4] {'ep'}, dimensions={0} | all-to-all | bytes 319488 | tf_op jit(solution)/shard_map/all_to_all | solution.py:43
  25.6 0.1 all_to_all.13
  25.7 7.8 %all_gather.3 = bf16[104,3072]{1,0:T(8,128)(2,1)S(1)} all-gather(bf16[104,768]{1,0:T(8,128)(2,1)S(1)} %all_to_all.13), channel_id=1, replica_groups=mesh['ep'=8,'tp'=4] {'tp'}, dimensions={1}, use_global_device_ids=true | all-gather | bytes 798720 | tf_op jit(solution)/shard_map/all_gather | solution.py:44
  33.5 3.2 %fusion.12 = f32[104,768]{1,0:T(8,128)S(1)} fusion(bf16[104,3072]{1,0:T(8,128)(2,1)S(1)} %all_gather.3, bf16[1,3072,768]{2,1,0:T(8,128)(2,1)} %param.11), kind=kOutput, calls=%fused_computation.9 | convolution fusion | flops 490813440 | bytes 5677056 | tf_op jit(solution)/shard_map/dot_general | solution.py:45
  36.7 0.0 copy-start
  36.7 6.5 %fusion.9 = bf16[3072,104]{0,1:T(8,128)(2,1)} fusion(bf16[1,768,3072]{2,1,0:T(8,128)(2,1)} %param.13, f32[104,768]{1,0:T(8,128)S(1)} %fusion.12, bf16[104,3072]{1,0:T(8,128)(2,1)S(1)} %all_gather.3, bf16[1,3072,768]{2,1,0:T(8,128)(2,1)} %param.12), kind=kOutput, calls=%fused_computation.8 | convolution fusion | flops 982505472 | bytes 11034624 | tf_op jit(solution)/shard_map/dot_general | solution.py:51
  43.2 0.0 reduce-scatter.2.cloned.1.call-update
  43.2 0.1 mul.76
  43.3 0.0 copy-done
  43.4 0.1 copy.17
  43.4 20.2 %reduce-scatter.2.cloned.1.call-done = bf16[768,104]{0,1:T(8,128)(2,1)} async-done(((bf16[3072,104]{0,1:T(8,128)(2,1)}), bf16[768,104]{0,1:T(8,128)(2,1)}) %reduce-scatter.2.cloned.1.call-update) | async-done | bytes 159760 | tf_op jit(solution)/shard_map/reduce_scatter | solution.py:50
  63.7 1.3 %fusion.56 = bf16[8,768,13]{1,2,0:T(8,128)(2,1)} fusion(bf16[768,104]{0,1:T(8,128)(2,1)} %reduce-scatter.2.cloned.1.call-done), kind=kLoop, calls=%fused_computation.56 | loop fusion | bytes 44544
  65.0 1.4 %fusion.55 = bf16[8,768,13]{1,2,0:T(8,128)(2,1)} fusion(bf16[8,768,13]{1,2,0:T(8,128)(2,1)} %fusion.56, bf16[768,104]{0,1:T(8,128)(2,1)} %reduce-scatter.2.cloned.1.call-done), kind=kLoop, calls=%fused_computation.54 | loop fusion | bytes 49152
  66.4 1.4 %fusion.54 = bf16[8,768,13]{1,2,0:T(8,128)(2,1)} fusion(bf16[8,768,13]{1,2,0:T(8,128)(2,1)} %fusion.55, bf16[768,104]{0,1:T(8,128)(2,1)} %reduce-scatter.2.cloned.1.call-done), kind=kLoop, calls=%fused_computation.52 | loop fusion | bytes 49152
  67.8 1.4 %fusion.53 = bf16[8,768,13]{1,2,0:T(8,128)(2,1)} fusion(bf16[8,768,13]{1,2,0:T(8,128)(2,1)} %fusion.54, bf16[768,104]{0,1:T(8,128)(2,1)} %reduce-scatter.2.cloned.1.call-done), kind=kLoop, calls=%fused_computation.50 | loop fusion | bytes 49152
  69.1 1.4 %fusion.52 = bf16[8,768,13]{1,2,0:T(8,128)(2,1)} fusion(bf16[8,768,13]{1,2,0:T(8,128)(2,1)} %fusion.53, bf16[768,104]{0,1:T(8,128)(2,1)} %reduce-scatter.2.cloned.1.call-done), kind=kLoop, calls=%fused_computation.48 | loop fusion | bytes 49152
  70.5 1.4 %fusion.51 = bf16[8,768,13]{1,2,0:T(8,128)(2,1)} fusion(bf16[8,768,13]{1,2,0:T(8,128)(2,1)} %fusion.52, bf16[768,104]{0,1:T(8,128)(2,1)} %reduce-scatter.2.cloned.1.call-done), kind=kLoop, calls=%fused_computation.46 | loop fusion | bytes 49152
  71.9 1.4 %fusion.50 = bf16[8,768,13]{1,2,0:T(8,128)(2,1)} fusion(bf16[8,768,13]{1,2,0:T(8,128)(2,1)} %fusion.51, bf16[768,104]{0,1:T(8,128)(2,1)} %reduce-scatter.2.cloned.1.call-done), kind=kLoop, calls=%fused_computation.44 | loop fusion | bytes 49152
  73.3 1.4 %fusion.49 = bf16[8,768,13]{1,2,0:T(8,128)(2,1)} fusion(bf16[8,768,13]{1,2,0:T(8,128)(2,1)} %fusion.50, bf16[768,104]{0,1:T(8,128)(2,1)} %reduce-scatter.2.cloned.1.call-done), kind=kLoop, calls=%fused_computation.42 | loop fusion | bytes 49152 | tf_op jit(solution)/shard_map/stack | solution.py:60
  74.6 5.5 %all-to-all-start.1 = ((bf16[8,768,13]{1,2,0:T(8,128)(2,1)}), bf16[8,768,13]{1,2,0:T(8,128)(2,1)S(1)}, u32[]{:S(2)}, u32[]{:S(2)}) async-start(bf16[8,768,13]{1,2,0:T(8,128)(2,1)} %fusion.49), calls=%async_computation.2 | async-start | bytes 393216 | tf_op jit(solution)/shard_map/all_to_all | solution.py:61
  80.2 7.8 %all-to-all-done.1 = bf16[8,768,13]{1,2,0:T(8,128)(2,1)S(1)} async-done(((bf16[8,768,13]{1,2,0:T(8,128)(2,1)}), bf16[8,768,13]{1,2,0:T(8,128)(2,1)S(1)}, u32[]{:S(2)}, u32[]{:S(2)}) %all-to-all-start.1) | async-done | bytes 159776 | tf_op jit(solution)/shard_map/all_to_all | solution.py:61
  87.9 0.1 reshape.59
  88.0 0.8 gather_fusion
  88.8 0.1 reshape.60
  88.9 0.9 multiply_reduce_fusion
  (6 shorter events, 0.1 us)
Async XLA Ops:
  6.5 57.1 %reduce-scatter.2.cloned.1.call-start = ((), (), s32[]{:S(2)}) async-start(), calls=%async_computation.3 | async-start | bytes 798720 | tf_op jit(solution)/shard_map/reduce_scatter | solution.py:50
  36.7 6.7 %copy-start = (f32[24,4]{0,1:T(4,128)S(1)}, f32[24,4]{0,1:T(4,128)}, u32[]{:S(2)}) copy-start(f32[24,4]{0,1:T(4,128)} %param.10) | copy-start | bytes 1156
  74.6 13.3 %all-to-all-start.1 = ((bf16[8,768,13]{1,2,0:T(8,128)(2,1)}), bf16[8,768,13]{1,2,0:T(8,128)(2,1)S(1)}, u32[]{:S(2)}, u32[]{:S(2)}) async-start(bf16[8,768,13]{1,2,0:T(8,128)(2,1)} %fusion.49), calls=%async_computation.2 | async-start | bytes 393216 | tf_op jit(solution)/shard_map/all_to_all | solution.py:61
Sparse Core Ops, SparseCore 0:
  43.4 20.2 reduce-scatter.1
